TPU v7x, 128 devices: a whole 4x4x4 slice. The times are simulated.
128 devices in a mesh: gr: 2 (over z_hi), fs: 32 (over z_lo, y, x), tp: 2 (over core).
Axes of the slice: x: 4, y: 4, z: 4 (z_hi: 2, z_lo: 2; z = z_hi * 2 + z_lo), core: 2. Of those that a mesh axis runs over, the one named last changes fastest.
Arguments:
- tokens: bfloat16 [4, 2048, 2048], P(('gr', 'tp')), may hold values from -6 to 6
- gate_master: float32 [3, 2048, 7168], P(None, 'fs', ('gr', 'tp')), may hold values from -0.125 to 0.125
- up_master: float32 [3, 2048, 7168], P(None, 'fs', ('gr', 'tp')), may hold values from -0.125 to 0.125
- down_master: float32 [3, 7168, 2048], P(None, 'fs', ('gr', 'tp')), may hold values from -0.0625 to 0.0625
- norm_gain: float32 [2048], P('fs'), may hold values from 0.1 to 1.9
- route: int32 [4, 2048, 2], P(('gr', 'tp')), may hold values from 0 to 2, all different within a row
- route_weight: float32 [4, 2048, 2], P(('gr', 'tp')), may hold values from 0.05 to 1
Outputs:
- gate_out: bfloat16 [3, 2048, 7168], P(None, None, 'fs')
- up_out: bfloat16 [3, 2048, 7168], P(None, None, 'fs')
- down_out: bfloat16 [3, 7168, 2048], P(None, 'fs')
- mixed: bfloat16 [4, 2048, 2048], P(('gr', 'tp'), 'fs')
Inputs may be any that keep to these rules, and one draw needn't show every extreme that they name: `route`: each token names two different experts; every expert is named by some token.
All inputs are finite; a program needn't handle non-finite values.
Results may differ from a plain program's by a relative error of at most 0.024.
Values may be sent and summed in bfloat16 or wider, within the bound.
No kernel may reach another device: no remote copies, remote signals or barrier semaphores. Data moves between devices by JAX's collectives and lax.ppermute only.
A program may use at most 192 MiB of HBM per device.

v0:
```python
import jax
import jax.numpy as jnp
from jax import lax
from jax.sharding import Mesh
from jax.sharding import PartitionSpec as P

FS = ("fs_0", "fs_1", "fs_2")


def reduced_to_own(blocks, axes, order):
    dims = [lax.axis_size(a) for a in axes]
    blocks = blocks.reshape(*dims, *blocks.shape[1:])
    blocks = blocks.transpose(*order, *range(len(axes), blocks.ndim))
    blocks = blocks.reshape(-1, *blocks.shape[len(axes) :])
    for k in order:
        blocks = lax.psum_scatter(blocks, axes[k], scatter_dimension=0, tiled=True)
    return blocks[0]


def split_up(array, dim, peers):
    dims = array.shape
    blocks = array.reshape(*dims[:dim], peers, dims[dim] // peers, *dims[dim + 1 :])
    return jnp.moveaxis(blocks, dim, 0)


def sum_by_axis_2(array, axes, order, dim):
    peers = lax.axis_size(axes)
    return reduced_to_own(split_up(array, dim, peers), axes, order)


def normalize(rows_in):
    values = rows_in.astype(jnp.float32)
    scaled = values * lax.rsqrt(jnp.mean(values * values, axis=-1, keepdims=True) + 1e-06)
    return scaled.astype(jnp.bfloat16)


def mixing(chosen, weights, experts):
    share = weights / jnp.sum(weights, axis=-1, keepdims=True)
    labels = jnp.arange(experts, dtype=jnp.int32)
    match = (chosen[:, :, None] == labels[None, None, :]).astype(jnp.float32)
    return jnp.sum(share[:, :, None] * match, axis=1)


def expert_term(normed, mix_column, gate_weight, up_weight, down_weight):
    gate_act = jnp.dot(normed, gate_weight, preferred_element_type=jnp.float32)
    up_act = jnp.dot(normed, up_weight, preferred_element_type=jnp.float32)
    hidden = (jax.nn.silu(gate_act) * up_act).astype(jnp.bfloat16)
    projected = jnp.dot(hidden, down_weight, preferred_element_type=jnp.float32)
    return mix_column * projected


def shards(tokens, gate_master, up_master, down_master, norm_gain, route, route_weight):
    scaled_gain = norm_gain[None, :, None]
    gate_local = (scaled_gain * gate_master).astype(jnp.bfloat16)
    up_local = (scaled_gain * up_master).astype(jnp.bfloat16)
    down_local = down_master.astype(jnp.bfloat16)
    experts = gate_local.shape[0]
    normed = normalize(tokens[0])
    combine = mixing(route[0], route_weight[0], experts)
    width = normed.shape[1]
    gate_rows, up_rows, down_out = (
        lax.all_gather(gate_local, ("gr", "tp"), axis=2, tiled=True),
        lax.all_gather(up_local, ("gr", "tp"), axis=2, tiled=True),
        lax.all_gather(down_local, ("gr", "tp"), axis=2, tiled=True),
    )
    gate_out, up_out = (
        lax.all_to_all(gate_rows, FS, split_axis=2, concat_axis=1, tiled=True),
        lax.all_to_all(up_rows, FS, split_axis=2, concat_axis=1, tiled=True),
    )
    own_rows = normed.shape[0] // lax.axis_size(FS)
    total = jnp.zeros((own_rows * lax.axis_size(FS), width), jnp.float32)
    for index in range(experts):
        total = total + expert_term(
            normed, combine[:, index : index + 1], gate_out[index], up_out[index], down_out[index]
        )
    summed = sum_by_axis_2(total.astype(jnp.bfloat16), FS, (1, 2, 0), 0).astype(jnp.float32)
    mixed = summed.astype(jnp.bfloat16)[None]
    return (gate_out, up_out, down_out, mixed)


def solution(mesh):
    split = Mesh(
        mesh.devices.reshape(mesh.shape["gr"], 2, 4, 4, mesh.shape["tp"]),
        ("gr", "fs_0", "fs_1", "fs_2", "tp"),
    )
    in_specs = (
        P(("gr", "tp"), None, None),
        P(None, FS, ("gr", "tp")),
        P(None, FS, ("gr", "tp")),
        P(None, FS, ("gr", "tp")),
        P(FS),
        P(("gr", "tp"), None, None),
        P(("gr", "tp"), None, None),
    )
    out_specs = (P(None, None, FS), P(None, None, FS), P(None, FS, None), P(("gr", "tp"), FS, None))
    return jax.shard_map(
        shards, mesh=split, in_specs=in_specs, out_specs=out_specs, check_vma=False
    )
```

profile of v0, /device:TPU:1, one launch (start us, length us, event | category | flops | bytes accessed | tf_op | source)
XLA Modules:
  0.0 390.9 jit_solution(5299467397481243480)
XLA Ops:
  11.1 33.5 %all-gather.4.cloned.1.call-done = bf16[3,64,7168]{2,1,0:T(8,128)(2,1)} async-done(((bf16[3,64,1792]{2,1,0:T(8,128)(2,1)}), bf16[3,64,7168]{2,1,0:T(8,128)(2,1)}) %all-gather.4.cloned.1.call-update) | async-done | bytes 2752528 | tf_op jit(solution)/shard_map/all_gather | solution.py:62
  44.5 10.1 %copy.41 = bf16[3,64,7168]{1,0,2:T(4,128)(2,1)} copy(bf16[3,64,7168]{2,1,0:T(8,128)(2,1)} %all-gather.4.cloned.1.call-done) | data formatting | bytes 5505024 | tf_op jit(solution)/shard_map/all_gather | solution.py:62
  54.6 12.6 %reshape.105 = bf16[32,2,21504]{2,1,0:T(2,128)(2,1)} reshape(bf16[7168,3,64]{2,1,0:T(4,128)(2,1)} %bitcast.55) | data formatting | bytes 5505024
  67.2 7.0 %all-to-all-start = ((bf16[32,2,21504]{2,1,0:T(2,128)(2,1)}), bf16[32,2,21504]{2,1,0:T(2,128)(2,1)S(1)}, u32[]{:S(2)}, u32[]{:S(2)}) async-start(bf16[32,2,21504]{2,1,0:T(2,128)(2,1)} %reshape.105), calls=%async_computation | async-start | bytes 5505024 | tf_op jit(solution)/shard_map/all_to_all | solution.py:67
  76.7 10.1 %copy.43 = bf16[3,64,7168]{1,0,2:T(4,128)(2,1)} copy(bf16[3,64,7168]{2,1,0:T(8,128)(2,1)} %all-gather.6.cloned.1.call-done) | data formatting | bytes 5505024 | tf_op jit(solution)/shard_map/all_gather | solution.py:63
  86.8 12.6 %reshape.107 = bf16[32,2,21504]{2,1,0:T(2,128)(2,1)} reshape(bf16[7168,3,64]{2,1,0:T(4,128)(2,1)} %bitcast.56) | data formatting | bytes 5505024
  99.4 9.2 %all-to-all-done = bf16[32,2,21504]{2,1,0:T(2,128)(2,1)S(1)} async-done(((bf16[32,2,21504]{2,1,0:T(2,128)(2,1)}), bf16[32,2,21504]{2,1,0:T(2,128)(2,1)S(1)}, u32[]{:S(2)}, u32[]{:S(2)}) %all-to-all-start) | async-done | bytes 2752544 | tf_op jit(solution)/shard_map/all_to_all | solution.py:67
  108.6 6.3 %all-to-all-start.1 = ((bf16[32,2,21504]{2,1,0:T(2,128)(2,1)}), bf16[32,2,21504]{2,1,0:T(2,128)(2,1)}, u32[]{:S(2)}, u32[]{:S(2)}) async-start(bf16[32,2,21504]{2,1,0:T(2,128)(2,1)} %reshape.107), calls=%async_computation.1 | async-start | bytes 5505024 | tf_op jit(solution)/shard_map/all_to_all | solution.py:68
  115.1 5.1 %fusion = f32[2048]{0:T(1024)S(1)} fusion(bf16[1,2048,2048]{2,1,0:T(8,128)(2,1)} %param.7), kind=kLoop, calls=%fused_computation.2 | loop fusion | flops 12580864 | bytes 8396800 | tf_op jit(solution)/shard_map/reduce_sum | solution.py:33
  120.3 8.0 %fusion.2 = bf16[2048,2048]{1,0:T(8,128)(2,1)} fusion(bf16[1,2048,2048]{2,1,0:T(8,128)(2,1)} %param.7, f32[2048]{0:T(1024)S(1)} %add_rsqrt_fusion), kind=kLoop, calls=%fused_computation.5 | loop fusion | flops 12582912 | bytes 16785408 | tf_op jit(solution)/shard_map/convert_element_type | solution.py:34
  128.3 8.7 %reshape.106 = bf16[7168,3,64]{2,1,0:T(4,128)(2,1)} reshape(bf16[32,2,21504]{2,1,0:T(2,128)(2,1)S(1)} %all-to-all-done) | data formatting | bytes 5505024
  136.9 10.7 %copy.42 = bf16[3,64,32,224]{3,1,2,0:T(8,128)(2,1)S(1)} copy(bf16[3,64,32,224]{1,0,3,2:T(4,128)(2,1)} %bitcast.57) | data formatting | bytes 5505024 | tf_op jit(solution)/shard_map/all_to_all | solution.py:67
  148.6 12.5 %reshape.108 = bf16[7168,3,64]{2,1,0:T(4,128)(2,1)} reshape(bf16[32,2,21504]{2,1,0:T(2,128)(2,1)} %all-to-all-done.1) | data formatting | bytes 5505024
  161.0 11.4 %copy.44 = bf16[3,64,32,224]{3,1,2,0:T(8,128)(2,1)} copy(bf16[3,64,32,224]{1,0,3,2:T(4,128)(2,1)} %bitcast.58) | data formatting | bytes 5505024 | tf_op jit(solution)/shard_map/all_to_all | solution.py:68
  176.1 8.0 %fusion.27 = f32[2048,224]{0,1:T(8,128)} fusion(bf16[2048,2048]{1,0:T(8,128)(2,1)} %fusion.2, bf16[2048,224]{1,0:T(8,128)(2,1)S(1)} %bitcast.68), kind=kOutput, calls=%fused_computation.41 | convolution fusion | flops 1879048192 | bytes 11141120 | tf_op jit(solution)/shard_map/dot_general | solution.py:45
  188.1 4.0 %fusion.29 = f32[2048,224]{0,1:T(8,128)} fusion(bf16[2048,2048]{1,0:T(8,128)(2,1)S(1)} %bitcast.52, bf16[2048,224]{1,0:T(8,128)(2,1)S(1)} %bitcast.66), kind=kOutput, calls=%fused_computation.43 | convolution fusion | flops 1879048192 | bytes 11141120 | tf_op jit(solution)/shard_map/dot_general | solution.py:45
  192.1 15.3 %fusion.7 = f32[2048,2048]{1,0:T(8,128)} fusion(bf16[2048,2048]{1,0:T(8,128)(2,1)} %fusion.2, bf16[2048,224]{1,0:T(8,128)(2,1)} %bitcast.64, f32[2048,224]{0,1:T(8,128)} %fusion.27, bf16[3,224,2048]{2,1,0:T(8,128)(2,1)} %all-gather.8.cloned.1.call-done), kind=kOutput, calls=%fused_computation.13 | convolution fusion | flops 3760848896 | bytes 28966912 | tf_op jit(solution)/shard_map/dot_general | solution.py:48
  207.4 15.5 %fusion.6 = f32[2048,2048]{1,0:T(8,128)} fusion(bf16[2048,2048]{1,0:T(8,128)(2,1)} %fusion.2, bf16[2048,224]{1,0:T(8,128)(2,1)} %bitcast.63, f32[2048,224]{0,1:T(8,128)} %fusion.28, bf16[3,224,2048]{2,1,0:T(8,128)(2,1)} %all-gather.8.cloned.1.call-done), kind=kOutput, calls=%fused_computation.12 | convolution fusion | flops 3760848896 | bytes 28966912 | tf_op jit(solution)/shard_map/dot_general | solution.py:48
  222.9 19.2 %add_convert_fusion = bf16[2048,2048]{1,0:T(8,128)(2,1)} fusion(f32[2048,2048]{1,0:T(8,128)} %fusion.6, f32[2048,2048]{1,0:T(8,128)} %fusion.7, f32[2048]{0:T(1024)S(1)} %bitcast.70, f32[2048]{0:T(1024)S(1)} %bitcast.71, f32[2048]{0:T(1024)S(1)} %bitcast.69, bf16[3,224,2048]{2,1,0:T(8,128)(2,1)} %all-gather.8.cloned.1.call-done, ...), kind=kOutput, calls=%fused_computation.4 | convolution fusion | flops 3786014720 | bytes 54157312 | tf_op jit(solution)/shard_map/dot_general | solution.py:48
  242.0 8.3 %copy.45 = bf16[4,4,2,64,2048]{4,3,2,1,0:T(8,128)(2,1)} copy(bf16[4,4,2,64,2048]{4,3,1,0,2:T(8,128)(2,1)} %bitcast.54) | data formatting | bytes 16777216 | tf_op jit(solution)/shard_map/transpose | solution.py:13
  250.4 80.8 %reduce-scatter.4.cloned.1.call-done = bf16[8,64,2048]{2,1,0:T(8,128)(2,1)} async-done(((bf16[32,64,2048]{2,1,0:T(8,128)(2,1)}), bf16[8,64,2048]{2,1,0:T(8,128)(2,1)}) %reduce-scatter.4.cloned.1.call-update) | async-done | bytes 2097168 | tf_op jit(solution)/shard_map/reduce_scatter | solution.py:16
  331.3 31.6 %reduce-scatter.6.cloned.1.call-done = bf16[2,64,2048]{2,1,0:T(8,128)(2,1)} async-done(((bf16[8,64,2048]{2,1,0:T(8,128)(2,1)}), bf16[2,64,2048]{2,1,0:T(8,128)(2,1)}) %reduce-scatter.6.cloned.1.call-update) | async-done | bytes 524304 | tf_op jit(solution)/shard_map/reduce_scatter | solution.py:16
  365.6 4.7 %copy.47 = bf16[3,2048,224]{1,2,0:T(8,128)(2,1)} copy(bf16[3,2048,224]{2,1,0:T(8,128)(2,1)} %bitcast.61) | data formatting | bytes 5505024
  370.3 12.2 %reduce-scatter.8.cloned.1.call-done = bf16[1,64,2048]{2,1,0:T(8,128)(2,1)} async-done(((bf16[2,64,2048]{2,1,0:T(8,128)(2,1)}), bf16[1,64,2048]{2,1,0:T(8,128)(2,1)}) %reduce-scatter.8.cloned.1.call-update) | async-done | bytes 262160 | tf_op jit(solution)/shard_map/reduce_scatter | solution.py:16
  (40 shorter events, 19.4 us)
Async XLA Ops:
  7.2 37.4 %all-gather.4.cloned.1.call-start = ((), (), s32[]{:S(2)}) async-start(), calls=%async_computation.5 | async-start | bytes 3440640 | tf_op jit(solution)/shard_map/all_gather | solution.py:62
  10.3 66.4 %all-gather.6.cloned.1.call-start = ((), (), s32[]{:S(2)}) async-start(), calls=%async_computation.6 | async-start | bytes 3440640 | tf_op jit(solution)/shard_map/all_gather | solution.py:63
  67.2 41.4 %all-to-all-start = ((bf16[32,2,21504]{2,1,0:T(2,128)(2,1)}), bf16[32,2,21504]{2,1,0:T(2,128)(2,1)S(1)}, u32[]{:S(2)}, u32[]{:S(2)}) async-start(bf16[32,2,21504]{2,1,0:T(2,128)(2,1)} %reshape.105), calls=%async_computation | async-start | bytes 5505024 | tf_op jit(solution)/shard_map/all_to_all | solution.py:67
  74.3 2.4 copy-start.2
  74.3 117.9 %all-gather.8.cloned.1.call-start = ((), (), s32[]{:S(2)}) async-start(), calls=%async_computation.7 | async-start | bytes 3440640 | tf_op jit(solution)/shard_map/all_gather | solution.py:64
  99.4 15.6 %copy-start.3 = (s32[1,2048,2]{1,2,0:T(2,128)S(1)}, s32[1,2048,2]{1,2,0:T(2,128)}, u32[]{:S(2)}) copy-start(s32[1,2048,2]{1,2,0:T(2,128)} %param.12) | copy-start | bytes 49156
  108.6 39.9 %all-to-all-start.1 = ((bf16[32,2,21504]{2,1,0:T(2,128)(2,1)}), bf16[32,2,21504]{2,1,0:T(2,128)(2,1)}, u32[]{:S(2)}, u32[]{:S(2)}) async-start(bf16[32,2,21504]{2,1,0:T(2,128)(2,1)} %reshape.107), calls=%async_computation.1 | async-start | bytes 5505024 | tf_op jit(solution)/shard_map/all_to_all | solution.py:68
  115.0 216.3 %reduce-scatter.4.cloned.1.call-start = ((), (), s32[]{:S(2)}) async-start(), calls=%async_computation.8 | async-start | bytes 10485760 | tf_op jit(solution)/shard_map/reduce_scatter | solution.py:16
  172.4 1.9 copy-start
  174.3 9.8 %slice-start = ((s8[8388608]{0:T(1024)(128)(4,1)}), s8[4194304]{0:T(1024)(128)(4,1)S(1)}, s32[]{:S(2)}) async-start(s8[8388608]{0:T(1024)(128)(4,1)} %bitcast.51), calls=%async_computation.11 | async-start | bytes 8388608
  176.1 8.0 %slice-start.1 = ((s8[8388608]{0:T(1024)(128)(4,1)}), s8[4194304]{0:T(1024)(128)(4,1)S(1)}, s32[]{:S(2)}) async-start(s8[8388608]{0:T(1024)(128)(4,1)} %bitcast.51), calls=%async_computation.12 | async-start | bytes 8388608
  250.3 112.5 %reduce-scatter.6.cloned.1.call-start = ((), (), s32[]{:S(2)}) async-start(), calls=%async_computation.9 | async-start | bytes 2621440 | tf_op jit(solution)/shard_map/reduce_scatter | solution.py:16
  331.2 51.3 %reduce-scatter.8.cloned.1.call-start = ((), (), s32[]{:S(2)}) async-start(), calls=%async_computation.10 | async-start | bytes 786432 | tf_op jit(solution)/shard_map/reduce_scatter | solution.py:16
  365.6 16.9 %copy-start.1 = (bf16[3,224,2048]{2,1,0:T(8,128)(2,1)S(1)}, bf16[3,224,2048]{2,1,0:T(8,128)(2,1)}, u32[]{:S(2)}) copy-start(bf16[3,224,2048]{2,1,0:T(8,128)(2,1)} %all-gather.8.cloned.1.call-done) | copy-start | bytes 8257540
Sparse Core Ops, SparseCore 0:
  10.4 34.0 all-gather.3
  46.8 29.6 all-gather.5
  78.1 74.4 all-gather.7
  250.5 80.7 reduce-scatter.3
  333.5 29.3 reduce-scatter.5
  365.6 16.8 reduce-scatter.7
where the time goes:
time: 393 us; the launch traced here: 391 us
  waiting for transfers between devices  169 us (43%)
  local copies, waits for them, and re-layouts  110 us (28%)
  matrix products  65.9 us (17%)
  other arithmetic  18.6 us (5%)
  between operations  14.2 us (4%)
  starting transfers between devices  13.6 us (3%)
    reduce_scatter x3, waiting for transfers between devices, reduced_to_own(): blocks = lax.psum_scatter(blocks, axes[k], scatter_dimension=0, tiled=True)  125 us
    unnamed x19, local copies, waits for them, and re-layouts  57 us
    dot_general x3, matrix products, expert_term(): projected = jnp.dot(hidden, down_weight, preferred_element_type=jnp.float32)  49.9 us
    all_gather x1, waiting for transfers between devices, shards(): lax.all_gather(gate_local, ('gr', 'tp'), axis=2, tiled=True)  33.5 us
    dot_general x3, matrix products, expert_term(): gate_act = jnp.dot(normed, gate_weight, preferred_element_type=jnp.float32)  16 us
    all_to_all x1, local copies, waits for them, and re-layouts, shards(): lax.all_to_all(up_rows, FS, split_axis=2, concat_axis=1, tiled=True)  11.4 us
    all_to_all x1, local copies, waits for them, and re-layouts, shards(): lax.all_to_all(gate_rows, FS, split_axis=2, concat_axis=1, tiled=True)  10.7 us
    all_gather x1, local copies, waits for them, and re-layouts, shards(): lax.all_gather(up_local, ('gr', 'tp'), axis=2, tiled=True)  10.1 us
  transfers between devices with their start and end apart: 8, of which 6 were waited for; matrix products, arithmetic and copies ran while one was open for 33% of the time, Pallas kernels for 0%

commit v1 on v0

--- a/solution.py
+++ b/solution.py
@@ -59,7 +59,7 @@
     combine = mixing(route[0], route_weight[0], experts)
     width = normed.shape[1]
     gate_rows, up_rows, down_out = (
-        lax.all_gather(gate_local, ("gr", "tp"), axis=2, tiled=True),
+        jnp.concatenate(lax.all_gather(gate_local, ("gr", "tp")), axis=2),
         lax.all_gather(up_local, ("gr", "tp"), axis=2, tiled=True),
         lax.all_gather(down_local, ("gr", "tp"), axis=2, tiled=True),
     )

time: 393 us -> 395 us (level)
  local copies, waits for them, and re-layouts: 110 us -> 123 us
  waiting for transfers between devices: 169 us -> 156 us
    reduce_scatter x3, waiting for transfers between devices: 125 us -> 113 us  [reduced_to_own(): blocks = lax.psum_scatter(blocks, axes[k], scatter_dimension=0, tiled=True)]
    reshape x0 -> x1, local copies, waits for them, and re-layouts: none -> 10.1 us  [shards(): jnp.concatenate(lax.all_gather(gate_local, ('gr', 'tp')), axis=2)]
    all_gather x1 -> x0, local copies, waits for them, and re-layouts: 10.1 us -> none  [shards(): lax.all_gather(gate_local, ('gr', 'tp'), axis=2, tiled=True)]
    all_to_all x1 -> x2, local copies, waits for them, and re-layouts: 10.7 us -> 19.4 us  [shards(): lax.all_to_all(gate_rows, FS, split_axis=2, concat_axis=1, tiled=True)]
    slice x1 -> x4, local copies, waits for them, and re-layouts: 0.22 us -> 5 us  [shards(): gate_out[index]]
    unnamed x19 -> x21, local copies, waits for them, and re-layouts: 57 us -> 57.4 us
  transfers between devices with their start and end apart: 8 -> 8, of which waited for: 6 -> 5; matrix products, arithmetic and copies ran while one was open for 33% -> 36% of each run, Pallas kernels for 0% -> 0%
where the time goes in v1:
time: 395 us; the launch traced here: 392 us
  waiting for transfers between devices  156 us (39%)
  local copies, waits for them, and re-layouts  123 us (31%)
  matrix products  66.3 us (17%)
  other arithmetic  18.7 us (5%)
  between operations  14.3 us (4%)
  starting transfers between devices  13.9 us (4%)
    reduce_scatter x3, waiting for transfers between devices, reduced_to_own(): blocks = lax.psum_scatter(blocks, axes[k], scatter_dimension=0, tiled=True)  113 us
    unnamed x21, local copies, waits for them, and re-layouts  57.4 us
    dot_general x3, matrix products, expert_term(): projected = jnp.dot(hidden, down_weight, preferred_element_type=jnp.float32)  50 us
    all_gather x1, waiting for transfers between devices, shards(): lax.all_gather(gate_local, ('gr', 'tp'))  33.5 us
    all_to_all x2, local copies, waits for them, and re-layouts, shards(): lax.all_to_all(gate_rows, FS, split_axis=2, concat_axis=1, tiled=True)  19.4 us
    dot_general x3, matrix products, expert_term(): gate_act = jnp.dot(normed, gate_weight, preferred_element_type=jnp.float32)  16.3 us
    all_to_all x1, local copies, waits for them, and re-layouts, shards(): lax.all_to_all(up_rows, FS, split_axis=2, concat_axis=1, tiled=True)  10.9 us
    reshape x1, local copies, waits for them, and re-layouts, shards(): jnp.concatenate(lax.all_gather(gate_local, ('gr', 'tp')), axis=2)  10.1 us
  transfers between devices with their start and end apart: 8, of which 5 were waited for; matrix products, arithmetic and copies ran while one was open for 36% of the time, Pallas kernels for 0%

profile of v1, /device:TPU:1, one launch (start us, length us, event | category | flops | bytes accessed | tf_op | source)
XLA Modules:
  0.0 392.5 jit_solution(5460865667643021811)
XLA Ops:
  11.1 33.5 %all-gather.9.cloned.1.call-done = bf16[12,64,1792]{2,1,0:T(8,128)(2,1)} async-done(((bf16[3,64,1792]{2,1,0:T(8,128)(2,1)}), bf16[12,64,1792]{2,1,0:T(8,128)(2,1)}) %all-gather.9.cloned.1.call-update) | async-done | bytes 2752528 | tf_op jit(solution)/shard_map/all_gather | solution.py:62
  44.5 10.1 %copy.55 = bf16[4,3,64,1792]{2,1,3,0:T(4,128)(2,1)} copy(bf16[4,3,64,1792]{3,2,1,0:T(8,128)(2,1)} %bitcast.73) | data formatting | bytes 5505024 | tf_op jit(solution)/shard_map/reshape | solution.py:62
  54.7 12.7 %reshape.114 = bf16[32,2,21504]{2,1,0:T(2,128)(2,1)} reshape(bf16[7168,3,64]{2,1,0:T(4,128)(2,1)} %bitcast.63) | data formatting | bytes 5505024
  67.4 6.9 %all-to-all-start = ((bf16[32,2,21504]{2,1,0:T(2,128)(2,1)}), bf16[32,2,21504]{2,1,0:T(2,128)(2,1)S(1)}, u32[]{:S(2)}, u32[]{:S(2)}) async-start(bf16[32,2,21504]{2,1,0:T(2,128)(2,1)} %reshape.114), calls=%async_computation | async-start | bytes 5505024 | tf_op jit(solution)/shard_map/all_to_all | solution.py:67
  76.9 10.1 %copy.44 = bf16[3,64,7168]{1,0,2:T(4,128)(2,1)} copy(bf16[3,64,7168]{2,1,0:T(8,128)(2,1)} %all-gather.5.cloned.1.call-done) | data formatting | bytes 5505024 | tf_op jit(solution)/shard_map/all_gather | solution.py:63
  87.0 12.6 %reshape.116 = bf16[32,2,21504]{2,1,0:T(2,128)(2,1)} reshape(bf16[7168,3,64]{2,1,0:T(4,128)(2,1)} %bitcast.64) | data formatting | bytes 5505024
  99.6 8.8 %all-to-all-done = bf16[32,2,21504]{2,1,0:T(2,128)(2,1)S(1)} async-done(((bf16[32,2,21504]{2,1,0:T(2,128)(2,1)}), bf16[32,2,21504]{2,1,0:T(2,128)(2,1)S(1)}, u32[]{:S(2)}, u32[]{:S(2)}) %all-to-all-start) | async-done | bytes 2752544 | tf_op jit(solution)/shard_map/all_to_all | solution.py:67
  108.4 6.8 %all-to-all-start.1 = ((bf16[32,2,21504]{2,1,0:T(2,128)(2,1)}), bf16[32,2,21504]{2,1,0:T(2,128)(2,1)}, u32[]{:S(2)}, u32[]{:S(2)}) async-start(bf16[32,2,21504]{2,1,0:T(2,128)(2,1)} %reshape.116), calls=%async_computation.1 | async-start | bytes 5505024 | tf_op jit(solution)/shard_map/all_to_all | solution.py:68
  115.3 5.1 %fusion = f32[2048]{0:T(1024)S(1)} fusion(bf16[1,2048,2048]{2,1,0:T(8,128)(2,1)} %param.7), kind=kLoop, calls=%fused_computation.2 | loop fusion | flops 12580864 | bytes 8396800 | tf_op jit(solution)/shard_map/reduce_sum | solution.py:33
  120.4 8.0 %fusion.2 = bf16[2048,2048]{1,0:T(8,128)(2,1)} fusion(bf16[1,2048,2048]{2,1,0:T(8,128)(2,1)} %param.7, f32[2048]{0:T(1024)S(1)} %add_rsqrt_fusion), kind=kLoop, calls=%fused_computation.5 | loop fusion | flops 12582912 | bytes 16785408 | tf_op jit(solution)/shard_map/convert_element_type | solution.py:34
  128.4 8.6 %reshape.115 = bf16[7168,3,64]{2,1,0:T(4,128)(2,1)} reshape(bf16[32,2,21504]{2,1,0:T(2,128)(2,1)S(1)} %all-to-all-done) | data formatting | bytes 5505024
  137.1 8.1 %copy.53 = bf16[3,64,32,224]{3,2,1,0:T(8,128)(2,1)S(1)} copy(bf16[3,64,32,224]{1,0,3,2:T(4,128)(2,1)} %bitcast.59) | data formatting | bytes 5505024 | tf_op jit(solution)/shard_map/all_to_all | solution.py:67
  150.1 12.4 %reshape.117 = bf16[7168,3,64]{2,1,0:T(4,128)(2,1)} reshape(bf16[32,2,21504]{2,1,0:T(2,128)(2,1)} %all-to-all-done.1) | data formatting | bytes 5505024
  162.6 10.9 %copy.45 = bf16[3,64,32,224]{3,1,2,0:T(8,128)(2,1)S(1)} copy(bf16[3,64,32,224]{1,0,3,2:T(4,128)(2,1)} %bitcast.65) | data formatting | bytes 5505024 | tf_op jit(solution)/shard_map/all_to_all | solution.py:68
  175.3 8.2 %fusion.29 = f32[2048,224]{0,1:T(8,128)} fusion(bf16[2048,2048]{1,0:T(8,128)(2,1)} %fusion.2, bf16[2048,224]{1,0:T(8,128)(2,1)S(1)} %bitcast.74), kind=kOutput, calls=%fused_computation.43 | convolution fusion | flops 1879048192 | bytes 11141120 | tf_op jit(solution)/shard_map/dot_general | solution.py:45
  183.5 4.0 %fusion.28 = f32[2048,224]{0,1:T(8,128)} fusion(bf16[2048,2048]{1,0:T(8,128)(2,1)S(1)} %bitcast.58, bf16[2048,224]{1,0:T(8,128)(2,1)S(1)} %bitcast.75), kind=kOutput, calls=%fused_computation.42 | convolution fusion | flops 1879048192 | bytes 11141120 | tf_op jit(solution)/shard_map/dot_general | solution.py:45
  191.6 15.3 %fusion.7 = f32[2048,2048]{1,0:T(8,128)} fusion(bf16[2048,2048]{1,0:T(8,128)(2,1)} %fusion.2, bf16[2048,224]{1,0:T(8,128)(2,1)} %bitcast.71, f32[2048,224]{0,1:T(8,128)} %fusion.27, bf16[3,224,2048]{2,1,0:T(8,128)(2,1)} %all-gather.7.cloned.1.call-done), kind=kOutput, calls=%fused_computation.13 | convolution fusion | flops 3760848896 | bytes 28966912 | tf_op jit(solution)/shard_map/dot_general | solution.py:48
  206.9 15.5 %fusion.6 = f32[2048,2048]{1,0:T(8,128)} fusion(bf16[2048,2048]{1,0:T(8,128)(2,1)} %fusion.2, bf16[2048,224]{1,0:T(8,128)(2,1)} %bitcast.70, f32[2048,224]{0,1:T(8,128)} %fusion.28, bf16[3,224,2048]{2,1,0:T(8,128)(2,1)} %all-gather.7.cloned.1.call-done), kind=kOutput, calls=%fused_computation.12 | convolution fusion | flops 3760848896 | bytes 28966912 | tf_op jit(solution)/shard_map/dot_general | solution.py:48
  222.3 19.3 %add_convert_fusion = bf16[2048,2048]{1,0:T(8,128)(2,1)} fusion(f32[2048,2048]{1,0:T(8,128)} %fusion.6, f32[2048,2048]{1,0:T(8,128)} %fusion.7, f32[2048]{0:T(1024)S(1)} %bitcast.78, f32[2048]{0:T(1024)S(1)} %bitcast.79, f32[2048]{0:T(1024)S(1)} %bitcast.77, bf16[3,224,2048]{2,1,0:T(8,128)(2,1)} %all-gather.7.cloned.1.call-done, ...), kind=kOutput, calls=%fused_computation.4 | convolution fusion | flops 3786014720 | bytes 54157312 | tf_op jit(solution)/shard_map/dot_general | solution.py:48
  241.6 8.3 %copy.49 = bf16[4,4,2,64,2048]{4,3,2,1,0:T(8,128)(2,1)} copy(bf16[4,4,2,64,2048]{4,3,1,0,2:T(8,128)(2,1)} %bitcast.62) | data formatting | bytes 16777216 | tf_op jit(solution)/shard_map/transpose | solution.py:13
  249.9 80.7 %reduce-scatter.4.cloned.1.call-done = bf16[8,64,2048]{2,1,0:T(8,128)(2,1)} async-done(((bf16[32,64,2048]{2,1,0:T(8,128)(2,1)}), bf16[8,64,2048]{2,1,0:T(8,128)(2,1)}) %reduce-scatter.4.cloned.1.call-update) | async-done | bytes 2097168 | tf_op jit(solution)/shard_map/reduce_scatter | solution.py:16
  330.7 31.6 %reduce-scatter.6.cloned.1.call-done = bf16[2,64,2048]{2,1,0:T(8,128)(2,1)} async-done(((bf16[8,64,2048]{2,1,0:T(8,128)(2,1)}), bf16[2,64,2048]{2,1,0:T(8,128)(2,1)}) %reduce-scatter.6.cloned.1.call-update) | async-done | bytes 524304 | tf_op jit(solution)/shard_map/reduce_scatter | solution.py:16
  362.3 11.4 %copy.54 = bf16[3,64,32,224]{3,1,2,0:T(8,128)(2,1)} copy(bf16[3,64,32,224]{1,0,3,2:T(4,128)(2,1)} %bitcast.60) | data formatting | bytes 5505024 | tf_op jit(solution)/shard_map/all_to_all | solution.py:67
  373.7 4.6 %copy.50 = bf16[3,2048,224]{1,2,0:T(8,128)(2,1)} copy(bf16[3,2048,224]{2,1,0:T(8,128)(2,1)} %bitcast.69) | data formatting | bytes 5505024
  (46 shorter events, 24.8 us)
Async XLA Ops:
  7.2 37.4 %all-gather.9.cloned.1.call-start = ((), (), s32[]{:S(2)}) async-start(), calls=%async_computation.10 | async-start | bytes 3440640 | tf_op jit(solution)/shard_map/all_gather | solution.py:62
  10.3 66.6 %all-gather.5.cloned.1.call-start = ((), (), s32[]{:S(2)}) async-start(), calls=%async_computation.5 | async-start | bytes 3440640 | tf_op jit(solution)/shard_map/all_gather | solution.py:63
  67.4 41.0 %all-to-all-start = ((bf16[32,2,21504]{2,1,0:T(2,128)(2,1)}), bf16[32,2,21504]{2,1,0:T(2,128)(2,1)S(1)}, u32[]{:S(2)}, u32[]{:S(2)}) async-start(bf16[32,2,21504]{2,1,0:T(2,128)(2,1)} %reshape.114), calls=%async_computation | async-start | bytes 5505024 | tf_op jit(solution)/shard_map/all_to_all | solution.py:67
  74.3 2.4 copy-start.3
  74.3 2.5 copy-start.4
  74.3 117.3 %all-gather.7.cloned.1.call-start = ((), (), s32[]{:S(2)}) async-start(), calls=%async_computation.6 | async-start | bytes 3440640 | tf_op jit(solution)/shard_map/all_gather | solution.py:64
  108.4 41.8 %all-to-all-start.1 = ((bf16[32,2,21504]{2,1,0:T(2,128)(2,1)}), bf16[32,2,21504]{2,1,0:T(2,128)(2,1)}, u32[]{:S(2)}, u32[]{:S(2)}) async-start(bf16[32,2,21504]{2,1,0:T(2,128)(2,1)} %reshape.116), calls=%async_computation.1 | async-start | bytes 5505024 | tf_op jit(solution)/shard_map/all_to_all | solution.py:68
  115.2 215.5 %reduce-scatter.4.cloned.1.call-start = ((), (), s32[]{:S(2)}) async-start(), calls=%async_computation.7 | async-start | bytes 10485760 | tf_op jit(solution)/shard_map/reduce_scatter | solution.py:16
  173.5 1.8 copy-start
  173.5 10.0 %slice-start = ((s8[8388608]{0:T(1024)(128)(4,1)}), s8[4194304]{0:T(1024)(128)(4,1)S(1)}, s32[]{:S(2)}) async-start(s8[8388608]{0:T(1024)(128)(4,1)} %bitcast.57), calls=%async_computation.11 | async-start | bytes 8388608
  175.3 8.2 %slice-start.1 = ((s8[8388608]{0:T(1024)(128)(4,1)}), s8[4194304]{0:T(1024)(128)(4,1)S(1)}, s32[]{:S(2)}) async-start(s8[8388608]{0:T(1024)(128)(4,1)} %bitcast.57), calls=%async_computation.12 | async-start | bytes 8388608
  175.3 8.2 %copy-start.1 = (bf16[1,32,64,224]{3,2,1,0:T(8,128)(2,1)S(1)}, bf16[1,32,64,224]{3,2,1,0:T(8,128)(2,1)}, u32[]{:S(2)}) copy-start(bf16[1,32,64,224]{3,2,1,0:T(8,128)(2,1)} %copy.47) | copy-start | bytes 2752516
  183.5 4.0 %copy-start.2 = (bf16[1,32,64,224]{3,2,1,0:T(8,128)(2,1)S(1)}, bf16[1,32,64,224]{3,2,1,0:T(8,128)(2,1)}, u32[]{:S(2)}) copy-start(bf16[1,32,64,224]{3,2,1,0:T(8,128)(2,1)} %copy.46) | copy-start | bytes 2752516
  249.9 112.4 %reduce-scatter.6.cloned.1.call-start = ((), (), s32[]{:S(2)}) async-start(), calls=%async_computation.8 | async-start | bytes 2621440 | tf_op jit(solution)/shard_map/reduce_scatter | solution.py:16
  330.7 51.3 %reduce-scatter.8.cloned.1.call-start = ((), (), s32[]{:S(2)}) async-start(), calls=%async_computation.9 | async-start | bytes 786432 | tf_op jit(solution)/shard_map/reduce_scatter | solution.py:16
Sparse Core Ops, SparseCore 0:
  10.4 34.0 all-gather.8
  46.8 29.6 all-gather.4
  78.1 74.5 all-gather.6
  250.0 80.5 reduce-scatter.3
  332.9 29.3 reduce-scatter.5
  365.1 16.8 reduce-scatter.7
